TPU v7x, 32 devices: a whole 2x2x4 slice. The times are simulated.
32 devices in a mesh: ep: 8 (over z, x), tp: 4 (over y, core).
Axes of the slice: x: 2, y: 2, z: 4, core: 2. Of those that a mesh axis runs over, the one named last changes fastest.
Arguments:
- x_attend: bfloat16 [4096, 2048], P('ep'), may hold values from -6 to 6
- attend_gain: float32 [2048], replicated, may hold values from 0.1 to 1.9
- w_query: bfloat16 [2048, 1024], P(None, 'tp'), may hold values from -0.125 to 0.125
- w_key: bfloat16 [2048, 512], P(None, 'tp'), may hold values from -0.125 to 0.125
- w_value: bfloat16 [2048, 512], P(None, 'tp'), may hold values from -0.125 to 0.125
- query_gain: float32 [64], replicated, may hold values from 0.1 to 1.9
- key_gain: float32 [64], replicated, may hold values from 0.1 to 1.9
- sink_logit: float32 [16], P('tp'), may hold values from 4 to 8
- w_output: bfloat16 [1024, 2048], P('tp'), may hold values from -1.5 to 1.5
- x_experts: bfloat16 [3072, 2048], P('ep'), may hold values from -6 to 6
- expert_gain: float32 [2048], replicated, may hold values from 0.1 to 1.9
- routes: int32 [3072, 2], P('ep'), may hold values from 0 to 7, all different within a row; in each aligned block of 384 rows (0 to 383, 384 to 767, ...) at most 144 rows name the same one
- group_prob: float32 [3072], P('ep'), may hold values from 0.3 to 1
- expert_prob: float32 [3072, 2], P('ep'), may hold values from 0.05 to 1
- w_gate: bfloat16 [8, 2048, 1024], P('ep', None, 'tp'), may hold values from -0.125 to 0.125
- w_up: bfloat16 [8, 2048, 1024], P('ep', None, 'tp'), may hold values from -0.125 to 0.125
- w_down: bfloat16 [8, 1024, 2048], P('ep', 'tp'), may hold values from -0.1875 to 0.1875
Outputs:
- attend_out: bfloat16 [4096, 2048], P(('ep', 'tp'))
- expert_out: bfloat16 [3072, 2048], P('ep', 'tp')
Inputs may be any that keep to these rules, and one draw needn't show every extreme that they name: `routes`: each row names 2 different experts. Among the rows of one device no expert is named more than 144 times, and in every draw some expert is named exactly 144 times by one device's rows.
All inputs are finite; a program needn't handle non-finite values.
Results may differ from a plain program's by a relative error of at most 0.012.
Values may be sent and summed in bfloat16 or wider, within the bound.
A program may use at most 64 MiB of HBM per device.

v0:
```python
import jax
import jax.numpy as jnp
from jax import lax
from jax.sharding import PartitionSpec as P

HEAD_DIM = 64
WINDOW = 128
GRID_W = 64
epsilon = 1e-06
rope_base = 10000.0


def extended(x, sides, width):
    for axis, dim in sides:
        peers, length = (lax.axis_size(axis), x.shape[dim])
        up = [(i, (i + 1) % peers) for i in range(peers - 1)]
        down = [(j, i) for i, j in up]
        last = lax.slice_in_dim(x, length - width, length, axis=dim)
        initial = lax.slice_in_dim(x, 0, width, axis=dim)
        before = lax.ppermute(last, axis, up)
        after = lax.ppermute(initial, axis, down)
        x = jnp.concatenate([before, x, after], axis=dim)
    return x


def rms_scale(inputs, gain):
    values_f = inputs.astype(jnp.float32)
    scaled = values_f * lax.rsqrt(jnp.mean(values_f * values_f, axis=-1, keepdims=True) + epsilon)
    return (scaled * gain).astype(jnp.bfloat16)


def rope_tables(positions):
    grid_rows = (positions // GRID_W).astype(jnp.float32)
    grid_cols = (positions % GRID_W).astype(jnp.float32)
    half_dim = HEAD_DIM // 2
    inverse = rope_base ** (-jnp.arange(0, half_dim, 2, dtype=jnp.float32) / half_dim)
    angles = jnp.concatenate([grid_rows[:, None] * inverse, grid_cols[:, None] * inverse], axis=-1)
    return (jnp.cos(angles), jnp.sin(angles))


def head_norm_rope(projected, gain, cosine, sine_tab):
    scaled = (
        projected
        * lax.rsqrt(jnp.mean(projected * projected, axis=-1, keepdims=True) + epsilon)
        * gain
    )
    first_half, second_half = jnp.split(scaled, 2, axis=-1)
    cos_b = cosine[:, None, :]
    sin_b = sine_tab[:, None, :]
    turned = jnp.concatenate(
        [first_half * cos_b - second_half * sin_b, second_half * cos_b + first_half * sin_b],
        axis=-1,
    )
    return turned.astype(jnp.bfloat16)


def per_device(
    x_attend,
    attend_gain,
    w_query,
    w_key,
    w_value,
    query_gain,
    key_gain,
    sink_logit,
    w_output,
    x_experts,
    expert_gain,
    routes,
    group_prob,
    expert_prob,
    w_gate,
    w_up,
    w_down,
):
    tok_rows = x_attend.shape[0]
    model_width = x_attend.shape[1]
    heads_local = sink_logit.shape[0]
    kv_local = w_key.shape[1] // HEAD_DIM
    group = heads_local // kv_local
    offset = lax.axis_index("ep") * tok_rows
    positions = offset + jnp.arange(tok_rows, dtype=jnp.int32)
    cosine, sine_tab = rope_tables(positions)
    normed = rms_scale(x_attend, attend_gain)
    queries = head_norm_rope(
        jnp.dot(normed, w_query, preferred_element_type=jnp.float32).reshape(
            tok_rows, heads_local, HEAD_DIM
        ),
        query_gain,
        cosine,
        sine_tab,
    )
    key_rows = head_norm_rope(
        jnp.dot(normed, w_key, preferred_element_type=jnp.float32).reshape(
            tok_rows, kv_local, HEAD_DIM
        ),
        key_gain,
        cosine,
        sine_tab,
    )
    values = jnp.dot(normed, w_value, preferred_element_type=jnp.float32).astype(jnp.bfloat16)
    stacked = jnp.stack([key_rows.reshape(tok_rows, kv_local * HEAD_DIM), values], axis=0)
    padded = extended(stacked, (("ep", 1),), WINDOW)
    span_keys = padded[0].reshape(tok_rows + 2 * WINDOW, kv_local, HEAD_DIM)
    span_values = padded[1].reshape(tok_rows + 2 * WINDOW, kv_local, HEAD_DIM)
    scores = jnp.einsum(
        "qhgd,khd->hgqk",
        queries.reshape(tok_rows, kv_local, group, HEAD_DIM),
        span_keys,
        preferred_element_type=jnp.float32,
    ) * HEAD_DIM ** (-0.5)
    key_pos = offset - WINDOW + jnp.arange(tok_rows + 2 * WINDOW, dtype=jnp.int32)
    total_len = tok_rows * lax.axis_size("ep")
    in_window = (
        (jnp.abs(positions[:, None] - key_pos[None, :]) <= WINDOW)
        & (key_pos[None, :] >= 0)
        & (key_pos[None, :] < total_len)
    )
    scores = jnp.where(in_window[None, None], scores, -1e30)
    sink_col = sink_logit.reshape(kv_local, group)[:, :, None]
    peak = jnp.maximum(jnp.max(scores, axis=-1), sink_col)[..., None]
    weights = jnp.exp(scores - peak)
    denominator = jnp.sum(weights, axis=-1, keepdims=True) + jnp.exp(sink_col[..., None] - peak)
    probs = (weights / denominator).astype(jnp.bfloat16)
    attended = jnp.einsum("hgqk,khd->qhgd", probs, span_values, preferred_element_type=jnp.float32)
    attended = attended.astype(jnp.bfloat16).reshape(tok_rows, heads_local * HEAD_DIM)
    rows_in = attended
    attend_out = lax.psum_scatter(
        jnp.dot(rows_in, w_output, preferred_element_type=jnp.float32).astype(jnp.bfloat16),
        "tp",
        scatter_dimension=0,
        tiled=True,
    )
    moe_rows = x_experts.shape[0]
    top_count = routes.shape[1]
    experts_n = lax.axis_size("ep")
    tp_count = lax.axis_size("tp")
    capacity = max(2, (3 * moe_rows * top_count + 2 * experts_n - 1) // (2 * experts_n))
    moe_normed = rms_scale(x_experts, expert_gain)
    flat_ids = routes.reshape(-1)
    onehot = (flat_ids[:, None] == jnp.arange(experts_n, dtype=jnp.int32)[None, :]).astype(
        jnp.int32
    )
    rank_in = jnp.cumsum(onehot, axis=0) - onehot
    slot_pos = jnp.sum(rank_in * onehot, axis=1)
    dest_slot = flat_ids * capacity + slot_pos
    owner_tok = jnp.arange(moe_rows * top_count, dtype=jnp.int32) // top_count
    slot_tok = jnp.full((experts_n * capacity,), moe_rows, jnp.int32).at[dest_slot].set(owner_tok)
    gate_mat = w_gate[0]
    up_mat = w_up[0]
    down_mat = w_down[0]
    col_width = model_width // tp_count
    own_cols = lax.dynamic_slice_in_dim(moe_normed, lax.axis_index("tp") * col_width, col_width, 1)
    padded_rows = jnp.concatenate([own_cols, jnp.zeros((1, col_width), jnp.bfloat16)], axis=0)
    outgoing = padded_rows[slot_tok].reshape(experts_n, capacity, col_width)
    arrived = lax.all_to_all(outgoing, "ep", split_axis=0, concat_axis=0, tiled=True)
    col_piece = lax.all_gather(arrived, "tp", axis=2, tiled=True)
    rows_in = col_piece.reshape(experts_n * capacity, col_piece.shape[2])
    gate_act = jnp.dot(rows_in, gate_mat, preferred_element_type=jnp.float32)
    up_act = jnp.dot(rows_in, up_mat, preferred_element_type=jnp.float32)
    hidden = (jax.nn.silu(gate_act) * up_act).astype(jnp.bfloat16)
    partial_value = jnp.dot(hidden, down_mat, preferred_element_type=jnp.float32).astype(
        jnp.bfloat16
    )
    summed = (
        lax.psum_scatter(partial_value, "tp", scatter_dimension=1, tiled=True)
        .astype(jnp.float32)
        .astype(jnp.bfloat16)
    )
    summed = summed.reshape(experts_n, capacity, summed.shape[1])
    returned = lax.all_to_all(summed, "ep", split_axis=0, concat_axis=0, tiled=True)
    returned = returned.reshape(experts_n * capacity, returned.shape[2])
    picked = returned[dest_slot].astype(jnp.float32)
    route_weight = group_prob[:, None] * expert_prob / jnp.sum(expert_prob, axis=1, keepdims=True)
    expert_out = jnp.sum(
        picked.reshape(moe_rows, top_count, picked.shape[1]) * route_weight[:, :, None], axis=1
    )
    return (attend_out, expert_out.astype(jnp.bfloat16))


def solution(mesh):
    placed = (
        P("ep", None),
        P(),
        P(None, "tp"),
        P(None, "tp"),
        P(None, "tp"),
        P(),
        P(),
        P("tp"),
        P("tp", None),
        P("ep", None),
        P(),
        P("ep", None),
        P("ep"),
        P("ep", None),
        P("ep", None, "tp"),
        P("ep", None, "tp"),
        P("ep", "tp", None),
    )
    return jax.shard_map(
        per_device,
        mesh=mesh,
        in_specs=placed,
        out_specs=(P(("ep", "tp"), None), P("ep", "tp")),
        check_vma=False,
    )
```

profile of v0, /device:TPU:0, one launch (start us, length us, event | category | flops | bytes accessed | tf_op | source)
XLA Modules:
  0.0 207.4 jit_solution(12722982645366641306)
XLA Ops:
  7.2 0.0 copy-start
  7.2 0.0 all-gather.2.cloned.1.call-start
  7.2 3.6 %convert_element_type.89 = f32[384,2048]{1,0:T(8,128)} convert(bf16[384,2048]{1,0:T(8,128)(2,1)} %param.26) | non-fusion elementwise | flops 786432 | bytes 4718592 | tf_op jit(solution)/shard_map/convert_element_type | solution.py:27
  10.9 0.4 multiply_reduce_fusion
  11.2 0.1 copy.31
  11.4 0.1 eq.31
  11.5 0.1 eq.27
  11.7 1.7 reduce-window.6
  13.4 0.1 slice.30
  13.5 0.1 copy.33
  13.7 0.2 reduce-window.9
  13.8 0.1 copy.34
  13.9 0.1 copy.30
  14.1 0.2 mul.275
  14.2 0.1 fusion.31
  14.3 3.4 %scatter_custom_fusion = s32[1152]{0:T(1024)S(1)} fusion(s32[768]{0:T(1024)S(1)} %fusion.40, s32[768]{0:T(1024)S(1)} %add_select_fusion, s32[]{:T(128)} %constant.107.clone.1), kind=kCustom, calls=%fused_computation.78 | custom fusion | bytes 4612 | tf_op jit(solution)/shard_map/scatter | solution.py:148
  17.7 0.8 dynamic-slice
  18.5 1.3 fusion.22
  19.8 4.2 %gather_fusion = bf16[1152,512]{1,0:T(8,128)(2,1)S(1)} fusion(bf16[385,512]{1,0:T(8,128)(2,1)S(1)} %concatenate.36, s32[2048]{0:T(1024)S(1)} %pad_clamp_fusion), kind=kCustom, calls=%fused_computation | custom fusion | bytes 2363904 | tf_op jit(solution)/shard_map/gather | solution.py:155
  24.1 0.0 copy-start.9
  24.1 36.2 %all_to_all.10 = bf16[8,144,512]{2,1,0:T(8,128)(2,1)} all-to-all(bf16[8,144,512]{2,1,0:T(8,128)(2,1)S(1)} %bitcast.69), channel_id=1, replica_groups=mesh['ep'=8,'tp'=4] {'ep'}, dimensions={0} | all-to-all | bytes 2359296 | tf_op jit(solution)/shard_map/all_to_all | solution.py:156
  60.3 0.0 all-gather.2.cloned.1.call-update
  60.3 0.0 reduce-scatter.5.cloned.1.call-start
  60.4 36.2 %all-gather.2.cloned.1.call-done = bf16[8,144,2048]{2,1,0:T(8,128)(2,1)} async-done(((bf16[8,144,512]{2,1,0:T(8,128)(2,1)}), bf16[8,144,2048]{2,1,0:T(8,128)(2,1)}) %all-gather.2.cloned.1.call-update) | async-done | bytes 4718608 | tf_op jit(solution)/shard_map/all_gather | solution.py:157
  96.6 4.8 %fusion.19 = f32[1152,256]{1,0:T(8,128)} fusion(bf16[1152,2048]{1,0:T(8,128)(2,1)} %bitcast.79, bf16[1,2048,256]{2,1,0:T(8,128)(2,1)S(1)} %copy-done.9), kind=kOutput, calls=%fused_computation.33 | convolution fusion | flops 1207959552 | bytes 6946816 | tf_op jit(solution)/shard_map/dot_general | solution.py:159
  101.4 9.7 %convolution_convert_fusion = bf16[1152,2048]{1,0:T(8,128)(2,1)} fusion(bf16[1152,2048]{1,0:T(8,128)(2,1)} %bitcast.80, f32[1152,256]{1,0:T(8,128)} %fusion.19, bf16[1,256,2048]{2,1,0:T(8,128)(2,1)S(1)} %copy-done, bf16[1,2048,256]{2,1,0:T(8,128)(2,1)S(1)} %copy-done.10), kind=kOutput, calls=%fused_computation.3 | convolution fusion | flops 2420047872 | bytes 12713984 | tf_op jit(solution)/shard_map/dot_general | solution.py:162
  111.1 0.0 reduce-scatter.5.cloned.1.call-update
  111.2 0.0 reduce-scatter.3.cloned.1.call-start
  111.3 0.1 broadcast_multiply_fusion.1
  111.3 0.2 fusion.29
  111.6 1.2 copy-done.2
  112.7 0.5 fusion.2
  113.2 2.0 multiply_reduce_fusion.3
  115.3 0.1 multiply_multiply_fusion.1
  115.4 0.1 copy.26
  115.5 1.9 fusion.15
  117.4 0.0 copy-start.8
  117.4 0.7 pad_maximum_fusion.3
  118.1 3.9 %collective-permute-start = (bf16[2,128,128]{2,1,0:T(8,128)(2,1)}, bf16[2,128,128]{2,1,0:T(8,128)(2,1)}, u32[]{:S(2)}, u32[]{:S(2)}) collective-permute-start(bf16[2,128,128]{2,1,0:T(8,128)(2,1)} %get-tuple-element.8), channel_id=1, source_target_pairs={{0,4},{4,8},{8,12},{12,16},{16,20},{20,24},{24,28},{1,5},{5,9},{9,... | collective-permute-start | bytes 196616 | tf_op jit(solution)/shard_map/ppermute | solution.py:20
  122.0 1.5 collective-permute-start.1
  123.6 2.2 %multiply_reduce_fusion.2 = (f32[512,4]{0,1:T(4,128)S(1)}, f32[512,256]{0,1:T(8,128)S(1)}) fusion(bf16[2048,256]{1,0:T(8,128)(2,1)} %param.19, bf16[512,2048]{1,0:T(8,128)(2,1)S(1)} %copy-done.2, f32[2048]{0:T(1024)} %param.18, f32[512]{0:T(512)S(1)} %add_rsqrt_fusion.3), kind=kOutput, calls=%fused_computation.40 | convolution fusion | flops 541325312 | bytes 3688448 | tf_op jit(solution)/shard_map/dot_general | solution.py:86
  125.8 0.1 multiply_multiply_fusion
  125.9 0.1 subtract_convert_fusion
  126.0 0.8 fusion.8
  126.8 0.1 max.17
  126.9 1.6 collective-permute-done.1
  128.5 0.9 pad_maximum_fusion
  129.4 0.1 copy.28
  129.6 0.1 copy.27
  129.7 1.3 fusion.1
  131.0 0.1 broadcast_maximum_fusion
  131.1 1.4 fusion
  132.5 0.1 exponential_add_fusion
  132.6 0.0 copy-start.3
  132.6 1.9 fusion.9
  134.5 2.1 %convolution_convert_fusion.1 = bf16[512,2048]{1,0:T(8,128)(2,1)} fusion(bf16[512,256]{0,1:T(8,128)(2,1)S(1)} %bitcast.71, bf16[256,2048]{1,0:T(8,128)(2,1)S(1)} %copy-done.3), kind=kOutput, calls=%fused_computation.16 | convolution fusion | flops 537919488 | bytes 3407872 | tf_op jit(solution)/shard_map/dot_general | solution.py:129
  136.6 0.0 reduce-scatter.3.cloned.1.call-update
  136.7 22.5 %reduce-scatter.5.cloned.1.call-done = bf16[1152,512]{1,0:T(8,128)(2,1)} async-done(((bf16[1152,2048]{1,0:T(8,128)(2,1)}), bf16[1152,512]{1,0:T(8,128)(2,1)}) %reduce-scatter.5.cloned.1.call-update) | async-done | bytes 1179664 | tf_op jit(solution)/shard_map/reduce_scatter | solution.py:166
  159.2 5.5 %all-to-all-start.1 = ((bf16[8,144,512]{2,1,0:T(8,128)(2,1)}), bf16[8,144,512]{2,1,0:T(8,128)(2,1)S(1)}, u32[]{:S(2)}, u32[]{:S(2)}) async-start(bf16[8,144,512]{2,1,0:T(8,128)(2,1)} %bitcast.70), calls=%async_computation.3 | async-start | bytes 2359296 | tf_op jit(solution)/shard_map/all_to_all | solution.py:171
  164.7 0.8 copy.35
  165.5 27.5 %all-to-all-done.1 = bf16[8,144,512]{2,1,0:T(8,128)(2,1)S(1)} async-done(((bf16[8,144,512]{2,1,0:T(8,128)(2,1)}), bf16[8,144,512]{2,1,0:T(8,128)(2,1)S(1)}, u32[]{:S(2)}, u32[]{:S(2)}) %all-to-all-start.1) | async-done | bytes 1179680 | tf_op jit(solution)/shard_map/all_to_all | solution.py:171
  193.1 2.7 %gather_fusion.1 = bf16[768,512]{1,0:T(8,128)(2,1)S(1)} fusion(bf16[1152,512]{1,0:T(8,128)(2,1)S(1)} %bitcast.68, s32[1024]{0:T(1024)S(1)} %pad_clamp_fusion.1), kind=kCustom, calls=%fused_computation.1 | custom fusion | bytes 1575936 | tf_op jit(solution)/shard_map/gather | solution.py:173
  195.7 1.0 reshape.323
  196.7 4.1 %multiply_reduce_fusion.1 = bf16[384,512]{1,0:T(8,128)(2,1)} fusion(f32[384,2,512]{2,1,0:T(2,128)S(1)} %reshape.323, f32[384,2]{1,0:T(8,128)} %copy.35), kind=kLoop, calls=%fused_computation.19 | loop fusion | flops 589824 | bytes 1969152 | tf_op jit(solution)/shard_map/reduce_sum | solution.py:175
  (45 shorter events, 0.3 us)
Async XLA Ops:
  7.2 94.3 %copy-start = (bf16[1,256,2048]{2,1,0:T(8,128)(2,1)S(1)}, bf16[1,256,2048]{2,1,0:T(8,128)(2,1)}, u32[]{:S(2)}) copy-start(bf16[1,256,2048]{2,1,0:T(8,128)(2,1)} %param.33) | copy-start | bytes 3145732
  7.2 3.7 %copy-start.1 = (bf16[384,2048]{1,0:T(8,128)(2,1)S(1)}, bf16[384,2048]{1,0:T(8,128)(2,1)}, u32[]{:S(2)}) copy-start(bf16[384,2048]{1,0:T(8,128)(2,1)} %param.26) | copy-start | bytes 4718596
  7.2 89.4 %all-gather.2.cloned.1.call-start = ((), (), s32[]{:S(2)}) async-start(), calls=%async_computation.5 | async-start | bytes 5898240 | tf_op jit(solution)/shard_map/all_gather | solution.py:157
  7.2 4.0 %copy-start.5 = (s32[384,2]{0,1:T(2,128)S(1)}, s32[384,2]{0,1:T(2,128)}, u32[]{:S(2)}) copy-start(s32[384,2]{0,1:T(2,128)} %param.28) | copy-start | bytes 9220
  24.1 72.6 %copy-start.9 = (bf16[1,2048,256]{2,1,0:T(8,128)(2,1)S(1)}, bf16[1,2048,256]{2,1,0:T(8,128)(2,1)}, u32[]{:S(2)}) copy-start(bf16[1,2048,256]{2,1,0:T(8,128)(2,1)} %param.31) | copy-start | bytes 3145732
  60.3 98.8 %reduce-scatter.5.cloned.1.call-start = ((), (), s32[]{:S(2)}) async-start(), calls=%async_computation.6 | async-start | bytes 5898240 | tf_op jit(solution)/shard_map/reduce_scatter | solution.py:166
  96.6 4.8 %copy-start.10 = (bf16[1,2048,256]{2,1,0:T(8,128)(2,1)S(1)}, bf16[1,2048,256]{2,1,0:T(8,128)(2,1)}, u32[]{:S(2)}) copy-start(bf16[1,2048,256]{2,1,0:T(8,128)(2,1)} %param.32) | copy-start | bytes 3145732
  111.1 1.6 copy-start.2
  111.1 2.1 %copy-start.11 = (f32[2048]{0:T(1024)S(1)}, f32[2048]{0:T(1024)}, u32[]{:S(2)}) copy-start(f32[2048]{0:T(1024)} %param.18) | copy-start | bytes 24580
  111.2 89.7 %reduce-scatter.3.cloned.1.call-start = ((), (), s32[]{:S(2)}) async-start(), calls=%async_computation.4 | async-start | bytes 2621440 | tf_op jit(solution)/shard_map/reduce_scatter | solution.py:128
  112.7 2.5 %copy-start.7 = (f32[64]{0:T(128)S(1)}, f32[64]{0:T(128)}, u32[]{:S(2)}) copy-start(f32[64]{0:T(128)} %param.23) | copy-start | bytes 772
  117.4 8.4 %copy-start.8 = (f32[64]{0:T(128)S(1)}, f32[64]{0:T(128)}, u32[]{:S(2)}) copy-start(f32[64]{0:T(128)} %param.22) | copy-start | bytes 772
  118.1 8.8 %collective-permute-start = (bf16[2,128,128]{2,1,0:T(8,128)(2,1)}, bf16[2,128,128]{2,1,0:T(8,128)(2,1)}, u32[]{:S(2)}, u32[]{:S(2)}) collective-permute-start(bf16[2,128,128]{2,1,0:T(8,128)(2,1)} %get-tuple-element.8), channel_id=1, source_target_pairs={{0,4},{4,8},{8,12},{12,16},{16,20},{20,24},{24,28},{1,5},{5,9},{9,... | collective-permute-start | bytes 196616 | tf_op jit(solution)/shard_map/ppermute | solution.py:20
  122.0 6.5 %collective-permute-start.1 = (bf16[2,128,128]{2,1,0:T(8,128)(2,1)}, bf16[2,128,128]{2,1,0:T(8,128)(2,1)}, u32[]{:S(2)}, u32[]{:S(2)}) collective-permute-start(bf16[2,128,128]{2,1,0:T(8,128)(2,1)} %get-tuple-element.9), channel_id=1, source_target_pairs={{4,0},{8,4},{12,8},{16,12},{20,16},{24,20},{28,24},{5,1},{9,5},{13... | collective-permute-start | bytes 196616 | tf_op jit(solution)/shard_map/ppermute | solution.py:21
  123.5 3.2 %copy-start.12 = (f32[4]{0:T(128)S(1)}, f32[4]{0:T(128)}, u32[]{:S(2)}) copy-start(f32[4]{0:T(128)} %param.24) | copy-start | bytes 52
  132.6 2.0 copy-start.3
  136.6 28.0 %copy-start.4 = (f32[384,2]{0,1:T(2,128)S(1)}, f32[384,2]{0,1:T(2,128)}, u32[]{:S(2)}) copy-start(f32[384,2]{0,1:T(2,128)} %param.30) | copy-start | bytes 9220
  136.6 28.1 %copy-start.6 = (f32[384]{0:T(512)S(1)}, f32[384]{0:T(512)}, u32[]{:S(2)}) copy-start(f32[384]{0:T(512)} %param.29) | copy-start | bytes 4612
  159.2 33.9 %all-to-all-start.1 = ((bf16[8,144,512]{2,1,0:T(8,128)(2,1)}), bf16[8,144,512]{2,1,0:T(8,128)(2,1)S(1)}, u32[]{:S(2)}, u32[]{:S(2)}) async-start(bf16[8,144,512]{2,1,0:T(8,128)(2,1)} %bitcast.70), calls=%async_computation.3 | async-start | bytes 2359296 | tf_op jit(solution)/shard_map/all_to_all | solution.py:171
Sparse Core Ops, SparseCore 0:
  60.4 36.1 all-gather.1
  111.3 47.8 reduce-scatter.4
  162.3 31.1 reduce-scatter.2
where the time goes:
time: 208 us; the launch traced here: 207 us
  waiting for transfers between devices  88 us (42%)
  blocking collectives  36.2 us (17%)
  matrix products  25.9 us (12%)
  other arithmetic  16.5 us (8%)
  local copies, waits for them, and re-layouts  15.6 us (8%)
  between operations  14.2 us (7%)
  starting transfers between devices  11 us (5%)
    all_gather x1, waiting for transfers between devices, per_device(): col_piece = lax.all_gather(arrived, 'tp', axis=2, tiled=True)  36.2 us
    all_to_all x1, blocking collectives, per_device(): lax.all_to_all(outgoing, 'ep', split_axis=0, concat_axis=0, tiled=True)  36.2 us
    all_to_all x1, waiting for transfers between devices, per_device(): lax.all_to_all(summed, 'ep', split_axis=0, concat_axis=0, tiled=True)  27.5 us
    reduce_scatter x1, waiting for transfers between devices, per_device(): lax.psum_scatter(partial_value, 'tp', scatter_dimension=1, tiled=True)  22.5 us
    dot_general x1, matrix products, per_device(): jnp.dot(hidden, down_mat, preferred_element_type=jnp.float32)  9.69 us
    all_to_all x1, starting transfers between devices, per_device(): lax.all_to_all(summed, 'ep', split_axis=0, concat_axis=0, tiled=True)  5.52 us
    dot_general x1, matrix products, per_device(): gate_act = jnp.dot(rows_in, gate_mat, preferred_element_type=jnp.float32)  4.82 us
    gather x1, local copies, waits for them, and re-layouts, per_device(): outgoing = padded_rows[slot_tok].reshape(experts_n, capacity, col_width)  4.24 us
  transfers between devices with their start and end apart: 6, of which 4 were waited for; matrix products, arithmetic and copies ran while one was open for 12% of the time, Pallas kernels for 0%

commit v1 on v0

--- a/solution.py
+++ b/solution.py
@@ -153,7 +153,18 @@
     own_cols = lax.dynamic_slice_in_dim(moe_normed, lax.axis_index("tp") * col_width, col_width, 1)
     padded_rows = jnp.concatenate([own_cols, jnp.zeros((1, col_width), jnp.bfloat16)], axis=0)
     outgoing = padded_rows[slot_tok].reshape(experts_n, capacity, col_width)
-    arrived = lax.all_to_all(outgoing, "ep", split_axis=0, concat_axis=0, tiled=True)
+    ways, here = (lax.axis_size("ep"), lax.axis_index("ep"))
+    width_2 = outgoing.shape[0] // ways
+    shape = list(outgoing.shape)
+    shape[0] = width_2
+    height = shape[0]
+    shape[0] = height * ways
+    arrived = jnp.zeros(shape, outgoing.dtype)
+    for mask in range(ways):
+        part = lax.dynamic_slice_in_dim(outgoing, (here ^ mask) * width_2, width_2, axis=0)
+        if mask:
+            part = lax.ppermute(part, "ep", [(d, d ^ mask) for d in range(ways)])
+        arrived = lax.dynamic_update_slice_in_dim(arrived, part, (here ^ mask) * height, axis=0)
     col_piece = lax.all_gather(arrived, "tp", axis=2, tiled=True)
     rows_in = col_piece.reshape(experts_n * capacity, col_piece.shape[2])
     gate_act = jnp.dot(rows_in, gate_mat, preferred_element_type=jnp.float32)

time: 208 us -> 209 us (level)
  blocking collectives: 36.2 us -> 0 us
  waiting for transfers between devices: 88 us -> 106 us
  starting transfers between devices: 11 us -> 24.4 us
  local copies, waits for them, and re-layouts: 15.6 us -> 21.9 us
    all_to_all x1 -> x0, blocking collectives: 36.2 us -> none  [per_device(): lax.all_to_all(outgoing, 'ep', split_axis=0, concat_axis=0, tiled=True)]
    ppermute x0 -> x7, starting transfers between devices: none -> 13.3 us  [per_device(): part = lax.ppermute(part, 'ep', [(d, d ^ mask) for d in range(ways)])]
    ppermute x0 -> x7, waiting for transfers between devices: none -> 13 us  [per_device(): part = lax.ppermute(part, 'ep', [(d, d ^ mask) for d in range(ways)])]
    dynamic_update_slice x0 -> x7, local copies, waits for them, and re-layouts: none -> 4.65 us  [per_device(): lax.dynamic_update_slice_in_dim(arrived, part, (here ^ mask) * height, ax...]
    all_gather x1, waiting for transfers between devices: 36.2 us -> 40.3 us  [per_device(): col_piece = lax.all_gather(arrived, 'tp', axis=2, tiled=True)]
  transfers between devices with their start and end apart: 6 -> 13, of which waited for: 4 -> 6; matrix products, arithmetic and copies ran while one was open for 12% -> 14% of each run, Pallas kernels for 0% -> 0%
where the time goes in v1:
time: 209 us; the launch traced here: 208 us
  waiting for transfers between devices  106 us (51%)
  matrix products  24.8 us (12%)
  starting transfers between devices  24.4 us (12%)
  local copies, waits for them, and re-layouts  21.9 us (10%)
  other arithmetic  16.4 us (8%)
  between operations  14.3 us (7%)
    all_gather x1, waiting for transfers between devices, per_device(): col_piece = lax.all_gather(arrived, 'tp', axis=2, tiled=True)  40.3 us
    all_to_all x1, waiting for transfers between devices, per_device(): lax.all_to_all(summed, 'ep', split_axis=0, concat_axis=0, tiled=True)  27.6 us
    reduce_scatter x1, waiting for transfers between devices, per_device(): lax.psum_scatter(partial_value, 'tp', scatter_dimension=1, tiled=True)  23.5 us
    ppermute x7, starting transfers between devices, per_device(): part = lax.ppermute(part, 'ep', [(d, d ^ mask) for d in range(ways)])  13.3 us
    ppermute x7, waiting for transfers between devices, per_device(): part = lax.ppermute(part, 'ep', [(d, d ^ mask) for d in range(ways)])  13 us
    dot_general x1, matrix products, per_device(): jnp.dot(hidden, down_mat, preferred_element_type=jnp.float32)  9.68 us
    all_to_all x1, starting transfers between devices, per_device(): lax.all_to_all(summed, 'ep', split_axis=0, concat_axis=0, tiled=True)  5.5 us
    dot_general x1, matrix products, per_device(): gate_act = jnp.dot(rows_in, gate_mat, preferred_element_type=jnp.float32)  4.82 us
  transfers between devices with their start and end apart: 13, of which 6 were waited for; matrix products, arithmetic and copies ran while one was open for 14% of the time, Pallas kernels for 0%

profile of v1, /device:TPU:0, one launch (start us, length us, event | category | flops | bytes accessed | tf_op | source)
XLA Modules:
  0.0 208.1 jit_solution(14739808150016395222)
XLA Ops:
  7.3 3.6 %convert_element_type.89 = f32[384,2048]{1,0:T(8,128)} convert(bf16[384,2048]{1,0:T(8,128)(2,1)} %param.26) | non-fusion elementwise | flops 786432 | bytes 4718592 | tf_op jit(solution)/shard_map/convert_element_type | solution.py:27
  10.9 0.4 multiply_reduce_fusion
  11.3 0.1 copy.31
  11.4 0.1 eq.31
  11.6 0.1 eq.27
  11.8 1.7 reduce-window.6
  13.5 0.1 copy.33
  13.7 0.2 reduce-window.9
  13.9 0.1 copy.30
  14.1 0.2 mul.275
  14.2 0.1 fusion.29
  14.3 3.4 %scatter_custom_fusion = s32[1152]{0:T(1024)S(1)} fusion(s32[768]{0:T(1024)S(1)} %fusion.38, s32[768]{0:T(1024)S(1)} %add_select_fusion, s32[]{:T(128)} %constant.115.clone.1), kind=kCustom, calls=%fused_computation.88 | custom fusion | bytes 4612 | tf_op jit(solution)/shard_map/scatter | solution.py:148
  17.8 0.8 dynamic-slice
  18.6 1.3 fusion.20
  19.9 4.2 %gather_fusion = bf16[1152,512]{1,0:T(8,128)(2,1)S(1)} fusion(bf16[385,512]{1,0:T(8,128)(2,1)S(1)} %concatenate.36, s32[2048]{0:T(1024)S(1)} %pad_clamp_fusion), kind=kCustom, calls=%fused_computation | custom fusion | bytes 2363904 | tf_op jit(solution)/shard_map/gather | solution.py:155
  24.1 1.1 broadcast_in_dim.16
  25.2 0.7 constant_dynamic-slice_fusion
  26.0 3.0 %collective-permute-start.2 = (bf16[1,144,512]{2,1,0:T(8,128)(2,1)S(1)}, bf16[1,144,512]{2,1,0:T(8,128)(2,1)S(1)}, u32[]{:S(2)}, u32[]{:S(2)}) collective-permute-start(bf16[1,144,512]{2,1,0:T(8,128)(2,1)S(1)} %get-tuple-element.8), channel_id=1, source_target_pairs={{0,4},{4,0},{8,12},{12,8},{16,20},{20,16},{24,28},{28,24},{1,5},{5... | collective-permute-start | bytes 442376 | tf_op jit(solution)/shard_map/ppermute | solution.py:166
  28.9 1.6 collective-permute-start.3
  30.5 3.0 %collective-permute-start.5 = (bf16[1,144,512]{2,1,0:T(8,128)(2,1)S(1)}, bf16[1,144,512]{2,1,0:T(8,128)(2,1)S(1)}, u32[]{:S(2)}, u32[]{:S(2)}) collective-permute-start(bf16[1,144,512]{2,1,0:T(8,128)(2,1)S(1)} %get-tuple-element.5), channel_id=1, source_target_pairs={{0,16},{4,20},{8,24},{12,28},{16,0},{20,4},{24,8},{28,12},{1,17},{... | collective-permute-start | bytes 442376 | tf_op jit(solution)/shard_map/ppermute | solution.py:166
  33.5 1.3 collective-permute-start.6
  34.8 3.6 %collective-permute-start.7 = (bf16[1,144,512]{2,1,0:T(8,128)(2,1)S(1)}, bf16[1,144,512]{2,1,0:T(8,128)(2,1)S(1)}, u32[]{:S(2)}, u32[]{:S(2)}) collective-permute-start(bf16[1,144,512]{2,1,0:T(8,128)(2,1)S(1)} %get-tuple-element.3), channel_id=1, source_target_pairs={{0,24},{4,28},{8,16},{12,20},{16,8},{20,12},{24,0},{28,4},{1,25},{... | collective-permute-start | bytes 442376 | tf_op jit(solution)/shard_map/ppermute | solution.py:166
  38.4 0.7 constant_dynamic-update-slice_fusion.5
  39.1 1.8 collective-permute-done.3
  40.9 0.9 collective-permute-start.8
  41.8 0.7 constant_dynamic-update-slice_fusion.4
  42.5 0.7 constant_dynamic-update-slice_fusion.3
  43.2 0.7 constant_dynamic-update-slice_fusion.2
  43.8 11.2 %collective-permute-done.6 = bf16[1,144,512]{2,1,0:T(8,128)(2,1)S(1)} collective-permute-done((bf16[1,144,512]{2,1,0:T(8,128)(2,1)S(1)}, bf16[1,144,512]{2,1,0:T(8,128)(2,1)S(1)}, u32[]{:S(2)}, u32[]{:S(2)}) %collective-permute-start.6) | collective-permute-done | bytes 147488 | tf_op jit(solution)/shard_map/ppermute | solution.py:166
  55.0 0.7 constant_dynamic-update-slice_fusion.1
  55.7 0.7 constant_dynamic-update-slice_fusion
  56.3 0.7 constant_dynamic-update-slice_fusion.6
  57.1 40.3 %all-gather.2.cloned.1.call-done = bf16[8,144,2048]{2,1,0:T(8,128)(2,1)} async-done(((bf16[8,144,512]{2,1,0:T(8,128)(2,1)}), bf16[8,144,2048]{2,1,0:T(8,128)(2,1)}) %all-gather.2.cloned.1.call-update) | async-done | bytes 4718608 | tf_op jit(solution)/shard_map/all_gather | solution.py:168
  97.4 4.8 %fusion.17 = f32[1152,256]{1,0:T(8,128)} fusion(bf16[1152,2048]{1,0:T(8,128)(2,1)} %bitcast.82, bf16[1,2048,256]{2,1,0:T(8,128)(2,1)S(1)} %copy-done.9), kind=kOutput, calls=%fused_computation.28 | convolution fusion | flops 1207959552 | bytes 6946816 | tf_op jit(solution)/shard_map/dot_general | solution.py:170
  102.2 9.7 %convolution_convert_fusion = bf16[1152,2048]{1,0:T(8,128)(2,1)} fusion(bf16[1,256,2048]{2,1,0:T(8,128)(2,1)S(1)} %copy-done, f32[1152,256]{1,0:T(8,128)} %fusion.17, bf16[1152,2048]{1,0:T(8,128)(2,1)} %bitcast.83, bf16[1,2048,256]{2,1,0:T(8,128)(2,1)S(1)} %copy-done.10), kind=kOutput, calls=%fused_computation.3 | convolution fusion | flops 2420047872 | bytes 12713984 | tf_op jit(solution)/shard_map/dot_general | solution.py:173
  111.9 0.2 reduce-scatter.3.cloned.1.call-start
  112.3 0.2 fusion.27
  112.5 1.0 copy-done.2
  113.5 0.5 fusion.2
  114.0 1.0 multiply_reduce_fusion.3
  115.0 0.1 multiply_multiply_fusion.1
  115.2 0.1 copy.26
  115.3 1.8 fusion.9
  117.1 0.7 pad_maximum_fusion.3
  117.8 4.0 %collective-permute-start = (bf16[2,128,128]{2,1,0:T(8,128)(2,1)}, bf16[2,128,128]{2,1,0:T(8,128)(2,1)}, u32[]{:S(2)}, u32[]{:S(2)}) collective-permute-start(bf16[2,128,128]{2,1,0:T(8,128)(2,1)} %get-tuple-element.16), channel_id=1, source_target_pairs={{0,4},{4,8},{8,12},{12,16},{16,20},{20,24},{24,28},{1,5},{5,9},{9,... | collective-permute-start | bytes 196616 | tf_op jit(solution)/shard_map/ppermute | solution.py:20
  121.8 1.3 collective-permute-start.1
  123.1 2.2 %multiply_reduce_fusion.2 = (f32[512,4]{0,1:T(4,128)S(1)}, f32[512,256]{0,1:T(8,128)S(1)}) fusion(bf16[2048,256]{1,0:T(8,128)(2,1)} %param.19, bf16[512,2048]{1,0:T(8,128)(2,1)S(1)} %copy-done.2, f32[2048]{0:T(1024)S(1)} %copy-done.12, f32[512]{0:T(512)S(1)} %add_rsqrt_fusion.3), kind=kOutput, calls=%fused_computation.35 | convolution fusion | flops 541325312 | bytes 3688448 | tf_op jit(solution)/shard_map/dot_general | solution.py:86
  125.4 0.1 multiply_multiply_fusion
  125.6 0.8 fusion.7
  126.5 1.8 collective-permute-done.1
  128.2 0.9 pad_maximum_fusion
  129.2 0.1 copy.28
  129.3 0.1 copy.27
  129.5 1.3 fusion.1
  130.8 1.4 fusion
  132.3 1.9 fusion.8
  134.3 2.1 %convolution_convert_fusion.1 = bf16[512,2048]{1,0:T(8,128)(2,1)} fusion(bf16[512,256]{0,1:T(8,128)(2,1)S(1)} %bitcast.74, bf16[256,2048]{1,0:T(8,128)(2,1)S(1)} %copy-done.3), kind=kOutput, calls=%fused_computation.16 | convolution fusion | flops 537919488 | bytes 3407872 | tf_op jit(solution)/shard_map/dot_general | solution.py:129
  136.4 23.5 %reduce-scatter.5.cloned.1.call-done = bf16[1152,512]{1,0:T(8,128)(2,1)} async-done(((bf16[1152,2048]{1,0:T(8,128)(2,1)}), bf16[1152,512]{1,0:T(8,128)(2,1)}) %reduce-scatter.5.cloned.1.call-update) | async-done | bytes 1179664 | tf_op jit(solution)/shard_map/reduce_scatter | solution.py:177
  159.9 5.5 %all-to-all-start = ((bf16[8,144,512]{2,1,0:T(8,128)(2,1)}), bf16[8,144,512]{2,1,0:T(8,128)(2,1)S(1)}, u32[]{:S(2)}, u32[]{:S(2)}) async-start(bf16[8,144,512]{2,1,0:T(8,128)(2,1)} %bitcast.73), calls=%async_computation.2 | async-start | bytes 2359296 | tf_op jit(solution)/shard_map/all_to_all | solution.py:182
  165.4 0.8 copy.35
  166.3 27.6 %all-to-all-done = bf16[8,144,512]{2,1,0:T(8,128)(2,1)S(1)} async-done(((bf16[8,144,512]{2,1,0:T(8,128)(2,1)}), bf16[8,144,512]{2,1,0:T(8,128)(2,1)S(1)}, u32[]{:S(2)}, u32[]{:S(2)}) %all-to-all-start) | async-done | bytes 1179680 | tf_op jit(solution)/shard_map/all_to_all | solution.py:182
  193.8 2.7 %gather_fusion.1 = bf16[768,512]{1,0:T(8,128)(2,1)S(1)} fusion(bf16[1152,512]{1,0:T(8,128)(2,1)S(1)} %bitcast.71, s32[1024]{0:T(1024)S(1)} %pad_clamp_fusion.1), kind=kCustom, calls=%fused_computation.1 | custom fusion | bytes 1575936 | tf_op jit(solution)/shard_map/gather | solution.py:184
  196.5 1.0 reshape.323
  197.5 4.1 %multiply_reduce_fusion.1 = bf16[384,512]{1,0:T(8,128)(2,1)} fusion(f32[384,2,512]{2,1,0:T(2,128)S(1)} %reshape.323, f32[384,2]{1,0:T(8,128)} %copy.35), kind=kLoop, calls=%fused_computation.17 | loop fusion | flops 589824 | bytes 1969152 | tf_op jit(solution)/shard_map/reduce_sum | solution.py:186
  (69 shorter events, 1.0 us)
Async XLA Ops:
  7.2 95.1 %copy-start = (bf16[1,256,2048]{2,1,0:T(8,128)(2,1)S(1)}, bf16[1,256,2048]{2,1,0:T(8,128)(2,1)}, u32[]{:S(2)}) copy-start(bf16[1,256,2048]{2,1,0:T(8,128)(2,1)} %param.33) | copy-start | bytes 3145732
  7.2 90.2 %all-gather.2.cloned.1.call-start = ((), (), s32[]{:S(2)}) async-start(), calls=%async_computation.4 | async-start | bytes 5898240 | tf_op jit(solution)/shard_map/all_gather | solution.py:168
  7.3 3.6 %copy-start.1 = (bf16[384,2048]{1,0:T(8,128)(2,1)S(1)}, bf16[384,2048]{1,0:T(8,128)(2,1)}, u32[]{:S(2)}) copy-start(bf16[384,2048]{1,0:T(8,128)(2,1)} %param.26) | copy-start | bytes 4718596
  7.3 4.0 %copy-start.5 = (s32[384,2]{0,1:T(2,128)S(1)}, s32[384,2]{0,1:T(2,128)}, u32[]{:S(2)}) copy-start(s32[384,2]{0,1:T(2,128)} %param.28) | copy-start | bytes 9220
  26.0 71.4 %copy-start.9 = (bf16[1,2048,256]{2,1,0:T(8,128)(2,1)S(1)}, bf16[1,2048,256]{2,1,0:T(8,128)(2,1)}, u32[]{:S(2)}) copy-start(bf16[1,2048,256]{2,1,0:T(8,128)(2,1)} %param.31) | copy-start | bytes 3145732
  26.0 8.8 %collective-permute-start.2 = (bf16[1,144,512]{2,1,0:T(8,128)(2,1)S(1)}, bf16[1,144,512]{2,1,0:T(8,128)(2,1)S(1)}, u32[]{:S(2)}, u32[]{:S(2)}) collective-permute-start(bf16[1,144,512]{2,1,0:T(8,128)(2,1)S(1)} %get-tuple-element.8), channel_id=1, source_target_pairs={{0,4},{4,0},{8,12},{12,8},{16,20},{20,16},{24,28},{28,24},{1,5},{5... | collective-permute-start | bytes 442376 | tf_op jit(solution)/shard_map/ppermute | solution.py:166
  28.9 11.9 %collective-permute-start.3 = (bf16[1,144,512]{2,1,0:T(8,128)(2,1)S(1)}, bf16[1,144,512]{2,1,0:T(8,128)(2,1)S(1)}, u32[]{:S(2)}, u32[]{:S(2)}) collective-permute-start(bf16[1,144,512]{2,1,0:T(8,128)(2,1)S(1)} %get-tuple-element.7), channel_id=1, source_target_pairs={{0,8},{4,12},{8,0},{12,4},{16,24},{20,28},{24,16},{28,20},{1,9},{5... | collective-permute-start | bytes 442376 | tf_op jit(solution)/shard_map/ppermute | solution.py:166
  30.5 11.9 %collective-permute-start.4 = (bf16[1,144,512]{2,1,0:T(8,128)(2,1)S(1)}, bf16[1,144,512]{2,1,0:T(8,128)(2,1)S(1)}, u32[]{:S(2)}, u32[]{:S(2)}) collective-permute-start(bf16[1,144,512]{2,1,0:T(8,128)(2,1)S(1)} %get-tuple-element.6), channel_id=1, source_target_pairs={{0,12},{4,8},{8,4},{12,0},{16,28},{20,24},{24,20},{28,16},{1,13},{... | collective-permute-start | bytes 442376 | tf_op jit(solution)/shard_map/ppermute | solution.py:166
  30.5 12.6 %collective-permute-start.5 = (bf16[1,144,512]{2,1,0:T(8,128)(2,1)S(1)}, bf16[1,144,512]{2,1,0:T(8,128)(2,1)S(1)}, u32[]{:S(2)}, u32[]{:S(2)}) collective-permute-start(bf16[1,144,512]{2,1,0:T(8,128)(2,1)S(1)} %get-tuple-element.5), channel_id=1, source_target_pairs={{0,16},{4,20},{8,24},{12,28},{16,0},{20,4},{24,8},{28,12},{1,17},{... | collective-permute-start | bytes 442376 | tf_op jit(solution)/shard_map/ppermute | solution.py:166
  33.5 21.5 %collective-permute-start.6 = (bf16[1,144,512]{2,1,0:T(8,128)(2,1)S(1)}, bf16[1,144,512]{2,1,0:T(8,128)(2,1)S(1)}, u32[]{:S(2)}, u32[]{:S(2)}) collective-permute-start(bf16[1,144,512]{2,1,0:T(8,128)(2,1)S(1)} %get-tuple-element.4), channel_id=1, source_target_pairs={{0,20},{4,16},{8,28},{12,24},{16,4},{20,0},{24,12},{28,8},{1,21},{... | collective-permute-start | bytes 442376 | tf_op jit(solution)/shard_map/ppermute | solution.py:166
  34.8 20.9 %collective-permute-start.7 = (bf16[1,144,512]{2,1,0:T(8,128)(2,1)S(1)}, bf16[1,144,512]{2,1,0:T(8,128)(2,1)S(1)}, u32[]{:S(2)}, u32[]{:S(2)}) collective-permute-start(bf16[1,144,512]{2,1,0:T(8,128)(2,1)S(1)} %get-tuple-element.3), channel_id=1, source_target_pairs={{0,24},{4,28},{8,16},{12,20},{16,8},{20,12},{24,0},{28,4},{1,25},{... | collective-permute-start | bytes 442376 | tf_op jit(solution)/shard_map/ppermute | solution.py:166
  40.9 15.5 %collective-permute-start.8 = (bf16[1,144,512]{2,1,0:T(8,128)(2,1)S(1)}, bf16[1,144,512]{2,1,0:T(8,128)(2,1)S(1)}, u32[]{:S(2)}, u32[]{:S(2)}) collective-permute-start(bf16[1,144,512]{2,1,0:T(8,128)(2,1)S(1)} %get-tuple-element.2), channel_id=1, source_target_pairs={{0,28},{4,24},{8,20},{12,16},{16,12},{20,8},{24,4},{28,0},{1,29},{... | collective-permute-start | bytes 442376 | tf_op jit(solution)/shard_map/ppermute | solution.py:166
  57.0 102.9 %reduce-scatter.5.cloned.1.call-start = ((), (), s32[]{:S(2)}) async-start(), calls=%async_computation.5 | async-start | bytes 5898240 | tf_op jit(solution)/shard_map/reduce_scatter | solution.py:177
  97.4 4.8 %copy-start.10 = (bf16[1,2048,256]{2,1,0:T(8,128)(2,1)S(1)}, bf16[1,2048,256]{2,1,0:T(8,128)(2,1)}, u32[]{:S(2)}) copy-start(bf16[1,2048,256]{2,1,0:T(8,128)(2,1)} %param.32) | copy-start | bytes 3145732
  111.9 1.6 copy-start.2
  111.9 2.1 copy-start.12
  111.9 89.6 %reduce-scatter.3.cloned.1.call-start = ((), (), s32[]{:S(2)}) async-start(), calls=%async_computation.3 | async-start | bytes 2621440 | tf_op jit(solution)/shard_map/reduce_scatter | solution.py:128
  112.2 1.8 copy-start.11
  114.0 1.0 copy-start.7
  117.8 8.7 %collective-permute-start = (bf16[2,128,128]{2,1,0:T(8,128)(2,1)}, bf16[2,128,128]{2,1,0:T(8,128)(2,1)}, u32[]{:S(2)}, u32[]{:S(2)}) collective-permute-start(bf16[2,128,128]{2,1,0:T(8,128)(2,1)} %get-tuple-element.16), channel_id=1, source_target_pairs={{0,4},{4,8},{8,12},{12,16},{16,20},{20,24},{24,28},{1,5},{5,9},{9,... | collective-permute-start | bytes 196616 | tf_op jit(solution)/shard_map/ppermute | solution.py:20
  121.8 6.5 %collective-permute-start.1 = (bf16[2,128,128]{2,1,0:T(8,128)(2,1)}, bf16[2,128,128]{2,1,0:T(8,128)(2,1)}, u32[]{:S(2)}, u32[]{:S(2)}) collective-permute-start(bf16[2,128,128]{2,1,0:T(8,128)(2,1)} %get-tuple-element.17), channel_id=1, source_target_pairs={{4,0},{8,4},{12,8},{16,12},{20,16},{24,20},{28,24},{5,1},{9,5},{13... | collective-permute-start | bytes 196616 | tf_op jit(solution)/shard_map/ppermute | solution.py:21
  123.1 2.3 %copy-start.8 = (f32[64]{0:T(128)S(1)}, f32[64]{0:T(128)}, u32[]{:S(2)}) copy-start(f32[64]{0:T(128)} %param.22) | copy-start | bytes 772
  125.4 1.0 copy-start.13
  132.3 2.0 copy-start.3
  136.4 29.0 %copy-start.4 = (f32[384,2]{0,1:T(2,128)S(1)}, f32[384,2]{0,1:T(2,128)}, u32[]{:S(2)}) copy-start(f32[384,2]{0,1:T(2,128)} %param.30) | copy-start | bytes 9220
  136.4 29.1 %copy-start.6 = (f32[384]{0:T(512)S(1)}, f32[384]{0:T(512)}, u32[]{:S(2)}) copy-start(f32[384]{0:T(512)} %param.29) | copy-start | bytes 4612
  159.9 33.9 %all-to-all-start = ((bf16[8,144,512]{2,1,0:T(8,128)(2,1)}), bf16[8,144,512]{2,1,0:T(8,128)(2,1)S(1)}, u32[]{:S(2)}, u32[]{:S(2)}) async-start(bf16[8,144,512]{2,1,0:T(8,128)(2,1)} %bitcast.73), calls=%async_computation.2 | async-start | bytes 2359296 | tf_op jit(solution)/shard_map/all_to_all | solution.py:182
Sparse Core Ops, SparseCore 0:
  57.1 40.1 all-gather.1
  112.0 47.7 reduce-scatter.4
  163.0 31.1 reduce-scatter.2
